TPU v7x, 32 devices: a whole 2x2x4 slice. The times are simulated.
32 devices in a mesh: ep: 16 (over z, y, x), tp: 2 (over core).
Axes of the slice: x: 2, y: 2, z: 4, core: 2. Of those that a mesh axis runs over, the one named last changes fastest.
Arguments:
- tokens: bfloat16 [112, 2304], P('ep'), may hold values from -6 to 6
- attn_gain: bfloat16 [2304], replicated, may hold values from 0.099609375 to 1.8984375
- query_weight: bfloat16 [2304, 2048], P(None, 'tp'), may hold values from -0.125 to 0.125
- key_weight: bfloat16 [2304, 2048], P(None, 'tp'), may hold values from -0.125 to 0.125
- value_weight: bfloat16 [2304, 2048], P(None, 'tp'), may hold values from -0.125 to 0.125
- out_weight: bfloat16 [2304, 2048], P(None, 'tp'), may hold values from -0.125 to 0.125
- lambdas: float32 [16], P('tp'), may hold values from 0.3 to 0.8
- head_gain: bfloat16 [128], replicated, may hold values from 0.099609375 to 1.8984375
- cache_keys: bfloat16 [112, 1024, 16, 128], P('ep', None, 'tp'), may hold values from -1500 to 1500
- cache_values: bfloat16 [112, 1024, 16, 128], P('ep', None, 'tp'), may hold values from -6 to 6
- lengths: int32 [112], P('ep'), may hold values from 2 to 1024, as said below
- moe_gain: bfloat16 [2304], replicated, may hold values from 0.099609375 to 1.8984375
- gate_weight: bfloat16 [16, 2304, 1024], P('ep', None, 'tp'), may hold values from -0.125 to 0.125
- up_weight: bfloat16 [16, 2304, 1024], P('ep', None, 'tp'), may hold values from -0.125 to 0.125
- down_weight: bfloat16 [16, 1024, 2304], P('ep', 'tp'), may hold values from -0.1875 to 0.1875
- shared_gate: bfloat16 [2304, 1024], P(None, 'tp'), may hold values from -0.125 to 0.125
- shared_up: bfloat16 [2304, 1024], P(None, 'tp'), may hold values from -0.125 to 0.125
- shared_down: bfloat16 [1024, 2304], P('tp'), may hold values from -0.1875 to 0.1875
- expert_ids: int32 [112, 6], P('ep'), may hold values from 0 to 15, all different within a row; in each aligned block of 7 rows (0 to 6, 7 to 13, ...) at most 5 rows name the same one
- expert_weights: float32 [112, 6], P('ep'), may hold values from 0.2 to 1
Outputs:
- result: bfloat16 [112, 2304], P('ep', 'tp')
Inputs may be any that keep to these rules, and one draw needn't show every extreme that they name: `expert_ids`: each row names 6 different experts. Among the rows of one device (aligned blocks of 7 rows) no expert is named by more than 5 rows, a bound that some block reaches. `lengths`: some sequence has 1024 cached positions.
All inputs are finite; a program needn't handle non-finite values.
Results may differ from a plain program's by a relative error of at most 0.02.
Values may be sent and summed in bfloat16 or wider, within the bound.
A program may use at most 128 MiB of HBM per device.

v0:
```python
import jax
import jax.numpy as jnp
from jax import lax
from jax.sharding import PartitionSpec as P

epsilon = 1e-06


def rms_scale(values, gain):
    wide = values.astype(jnp.float32)
    return (
        wide
        * lax.rsqrt(jnp.mean(wide * wide, axis=-1, keepdims=True) + epsilon)
        * gain.astype(jnp.float32)
    )


def shards(
    tokens,
    attn_gain,
    query_weight,
    key_weight,
    value_weight,
    out_weight,
    lambdas,
    head_gain,
    cache_keys,
    cache_values,
    lengths,
    moe_gain,
    gate_weight,
    up_weight,
    down_weight,
    shared_gate,
    shared_up,
    shared_down,
    expert_ids,
    expert_weights,
):
    seq_dev, model_width = tokens.shape
    local_heads = lambdas.shape[0]
    head_dim = cache_keys.shape[-1] // 2
    cache_len = cache_keys.shape[1]
    normed = rms_scale(tokens, attn_gain).astype(jnp.bfloat16)
    query_rows = jnp.dot(normed, query_weight, preferred_element_type=jnp.float32).astype(
        jnp.bfloat16
    )
    key_new = jnp.dot(normed, key_weight, preferred_element_type=jnp.float32).astype(jnp.bfloat16)
    value_new = jnp.dot(normed, value_weight, preferred_element_type=jnp.float32).astype(
        jnp.bfloat16
    )
    score_scale = head_dim ** (-0.5)
    queries = query_rows.reshape(seq_dev, local_heads, 2, head_dim)
    new_keys = key_new.reshape(seq_dev, local_heads, 2, head_dim)
    new_values = value_new.reshape(seq_dev, local_heads, 2 * head_dim)
    past_keys = cache_keys.reshape(seq_dev, cache_len, local_heads, 2, head_dim)
    scores = (
        jnp.einsum("shmd,sjhmd->shmj", queries, past_keys, preferred_element_type=jnp.float32)
        * score_scale
    )
    own_score = (
        jnp.sum(queries.astype(jnp.float32) * new_keys.astype(jnp.float32), axis=-1) * score_scale
    )
    live_mask = (jnp.arange(cache_len, dtype=jnp.int32)[None, :] < lengths[:, None])[
        :, None, None, :
    ]
    peak_score = jnp.maximum(jnp.max(jnp.where(live_mask, scores, -jnp.inf), axis=-1), own_score)
    exp_terms = jnp.where(live_mask, jnp.exp(scores - peak_score[..., None]), 0.0)
    own_term = jnp.exp(own_score - peak_score)
    denom_sum = jnp.sum(exp_terms, axis=-1) + own_term
    map_probs = exp_terms / denom_sum[..., None]
    own_prob = own_term / denom_sum
    lambda_row = lambdas[None, :]
    mixture = (map_probs[:, :, 0] - lambda_row[..., None] * map_probs[:, :, 1]).astype(jnp.bfloat16)
    own_mixture = (own_prob[:, :, 0] - lambda_row * own_prob[:, :, 1]).astype(jnp.bfloat16)
    head_out = jnp.einsum(
        "shj,sjhv->shv", mixture, cache_values, preferred_element_type=jnp.float32
    )
    head_out = head_out + own_mixture.astype(jnp.float32)[..., None] * new_values.astype(
        jnp.float32
    )
    head_normed = (
        rms_scale(head_out, head_gain)
        .astype(jnp.bfloat16)
        .reshape(seq_dev, local_heads * 2 * head_dim)
    )
    attn_part = lax.dot_general(
        head_normed, out_weight, (((1,), (1,)), ((), ())), preferred_element_type=jnp.float32
    )
    attn_total = lax.psum(attn_part.astype(jnp.bfloat16), "tp").astype(jnp.float32)
    mixed_rows = (tokens.astype(jnp.float32) + attn_total).astype(jnp.bfloat16)
    moe_normed = rms_scale(mixed_rows, moe_gain).astype(jnp.bfloat16)
    shared_gate_out = jnp.dot(moe_normed, shared_gate, preferred_element_type=jnp.float32)
    shared_up_out = jnp.dot(moe_normed, shared_up, preferred_element_type=jnp.float32)
    shared_hidden = (jax.nn.silu(shared_gate_out) * shared_up_out).astype(jnp.bfloat16)
    shared_part = jnp.dot(shared_hidden, shared_down, preferred_element_type=jnp.float32)
    experts = lax.axis_size("ep")
    top_count = expert_ids.shape[1]
    capacity = min(seq_dev, max(2, 2 * seq_dev * top_count // experts))
    slot_count = seq_dev * top_count
    slot_ids = expert_ids.reshape(slot_count)
    expert_hits = (slot_ids[:, None] == jnp.arange(experts, dtype=jnp.int32)[None, :]).astype(
        jnp.int32
    )
    slot_rank = jnp.sum((jnp.cumsum(expert_hits, axis=0) - expert_hits) * expert_hits, axis=1)
    slot_place = slot_ids * capacity + slot_rank
    placed = (
        slot_place[:, None] == jnp.arange(experts * capacity, dtype=jnp.int32)[None, :]
    ).astype(jnp.bfloat16)
    slot_token = jnp.arange(slot_count, dtype=jnp.int32) // top_count
    token_pick = (slot_token[:, None] == jnp.arange(seq_dev, dtype=jnp.int32)[None, :]).astype(
        jnp.bfloat16
    )
    dispatch = lax.dot_general(
        placed, token_pick, (((0,), (0,)), ((), ())), preferred_element_type=jnp.float32
    ).astype(jnp.bfloat16)
    col_count = model_width // lax.axis_size("tp")
    own_start = lax.axis_index("tp") * col_count
    own_normed = lax.dynamic_slice_in_dim(moe_normed, own_start, col_count, 1)
    send_slice = jnp.dot(dispatch, own_normed, preferred_element_type=jnp.float32).astype(
        jnp.bfloat16
    )
    arrived = lax.all_to_all(send_slice, "ep", split_axis=0, concat_axis=0, tiled=True)
    received = lax.all_gather(arrived, "tp", axis=1, tiled=True)
    gate_out = jnp.dot(received, gate_weight[0], preferred_element_type=jnp.float32)
    up_out = jnp.dot(received, up_weight[0], preferred_element_type=jnp.float32)
    expert_hidden = (jax.nn.silu(gate_out) * up_out).astype(jnp.bfloat16)
    expert_part = jnp.dot(expert_hidden, down_weight[0], preferred_element_type=jnp.float32)
    expert_sum, shared_out = (
        lax.psum_scatter(
            expert_part.astype(jnp.bfloat16), "tp", scatter_dimension=1, tiled=True
        ).astype(jnp.float32),
        lax.psum_scatter(
            shared_part.astype(jnp.bfloat16), "tp", scatter_dimension=1, tiled=True
        ).astype(jnp.float32),
    )
    returned = lax.all_to_all(
        expert_sum.astype(jnp.bfloat16), "ep", split_axis=0, concat_axis=0, tiled=True
    )
    slot_values = jnp.dot(placed, returned, preferred_element_type=jnp.float32).reshape(
        seq_dev, top_count, col_count
    )
    routed = jnp.sum(expert_weights[:, :, None] * slot_values, axis=1)
    own_cols = lax.dynamic_slice_in_dim(mixed_rows, own_start, col_count, 1)
    return (own_cols.astype(jnp.float32) + routed + shared_out).astype(jnp.bfloat16)


def solution(mesh):
    in_specs = (
        P("ep", None),
        P(),
        P(None, "tp"),
        P(None, "tp"),
        P(None, "tp"),
        P(None, "tp"),
        P("tp"),
        P(),
        P("ep", None, "tp", None),
        P("ep", None, "tp", None),
        P("ep"),
        P(),
        P("ep", None, "tp"),
        P("ep", None, "tp"),
        P("ep", "tp", None),
        P(None, "tp"),
        P(None, "tp"),
        P("tp", None),
        P("ep", None),
        P("ep", None),
    )
    out_specs = P("ep", "tp")
    return jax.shard_map(shards, mesh=mesh, in_specs=in_specs, out_specs=out_specs, check_vma=False)
```

profile of v0, /device:TPU:0, one launch (start us, length us, event | category | flops | bytes accessed | tf_op | source)
XLA Modules:
  0.0 123.7 jit_solution(13733338271488698938)
XLA Ops:
  6.5 0.0 copy-start
  6.5 0.8 convert_element_type.102
  7.4 0.9 fusion.36
  8.3 3.1 %convolution_convert_fusion.6 = bf16[7,1024]{1,0:T(8,128)(2,1)S(1)} fusion(bf16[2304,1024]{1,0:T(8,128)(2,1)} %param.22, bf16[7,2304]{1,0:T(8,128)(2,1)} %param.20, f32[2304]{0:T(1024)S(1)} %convert_element_type.102, f32[7]{0:T(128)S(1)} %add_rsqrt_fusion.2), kind=kOutput, calls=%fused_computation.20 | convolution fusion | flops 33101824 | bytes 4774428 | tf_op jit(solution)/shard_map/dot_general | solution.py:45
  11.4 0.1 reshape.146
  11.5 0.1 reshape.134
  11.6 0.0 copy-start.1
  11.6 20.6 %copy.40 = bf16[7,1024,8,128]{1,3,2,0:T(8,128)(2,1)} copy(bf16[7,1024,8,128]{3,2,1,0:T(8,128)(2,1)} %param.28) | data formatting | bytes 29360128 | tf_op args[8]
  32.2 0.1 iota_compare_fusion
  32.3 3.1 %fusion.18 = f32[7,1024]{1,0:T(8,128)S(1)} fusion(bf16[2304,1024]{1,0:T(8,128)(2,1)} %param.23, bf16[7,2304]{1,0:T(8,128)(2,1)S(1)} %copy-done.1, f32[2304]{0:T(1024)S(1)} %convert_element_type.102, f32[7]{0:T(128)S(1)} %add_rsqrt_fusion.2), kind=kOutput, calls=%fused_computation.19 | convolution fusion | flops 33108992 | bytes 4788764 | tf_op jit(solution)/shard_map/dot_general | solution.py:48
  35.4 0.1 reshape.137
  35.5 0.1 multiply_reduce_fusion
  35.7 0.1 copy.41
  35.8 7.3 %fusion.69 = f32[7,8,2,1,1024]{4,3,2,1,0:T(1,128)S(1)} fusion(bf16[7,8,2,64,1]{3,4,2,1,0:T(2,128)(2,1)S(1)} %reshape.146, bf16[7,1024,8,2,64]{1,4,3,2,0:T(8,128)(2,1)} %bitcast.87), kind=kOutput, calls=%fused_computation.101 | convolution fusion | flops 14680064 | bytes 15153152 | tf_op jit(solution)/shard_map/shmd,sjhmd->shmj/dot_general | solution.py:58
  43.1 0.3 select_reduce_fusion
  43.4 0.3 fusion.21
  43.7 0.2 fusion.20
  44.0 0.1 fusion.31
  44.1 0.0 slice-done
  44.1 0.0 slice-done.1
  44.2 0.0 slice-start.2
  44.2 0.8 fusion.17
  44.9 7.6 %fusion = f32[7,8,1,128]{3,2,1,0:T(1,128)S(1)} fusion(bf16[7,1024,8,128]{3,2,1,0:T(8,128)(2,1)} %param.29, bf16[7,8,1024,1]{2,1,0,3:T(8,128)(2,1)S(1)} %fusion.31), kind=kOutput, calls=%fused_computation | convolution fusion | flops 14680064 | bytes 14823424 | tf_op jit(solution)/shard_map/shj,sjhv->shv/dot_general | solution.py:76
  52.6 0.0 copy-start.3
  52.6 0.0 copy-start.2
  52.6 0.2 multiply_reduce_fusion.1
  52.8 0.1 fusion.52
  52.8 0.0 slice-done.2
  52.9 1.3 %convolution_convert_fusion.2 = bf16[7,2304]{1,0:T(8,128)(2,1)S(1)} fusion(bf16[2304,1024]{1,0:T(8,128)(2,1)S(1)} %bitcast.91, bf16[1,7,8,128]{3,2,1,0:T(8,128)(2,1)S(1)} %fusion.52), kind=kOutput, calls=%fused_computation.4 | convolution fusion | flops 33046272 | bytes 4765184 | tf_op jit(solution)/shard_map/dot_general | solution.py:87
  54.2 3.8 %psum.7 = bf16[7,2304]{1,0:T(8,128)(2,1)S(1)} all-reduce(bf16[7,2304]{1,0:T(8,128)(2,1)S(1)} %convolution_convert_fusion.2), channel_id=1, replica_groups=mesh['ep'=16,'tp'=2] {'tp'}, use_global_device_ids=true, to_apply=%region_5.6 | all-reduce | flops 16128 | bytes 64512 | tf_op jit(solution)/shard_map/psum | solution.py:90
  58.0 0.1 fusion.33
  58.1 0.1 eq.63
  58.2 0.1 fusion.41
  58.3 0.1 reduce_window_sum.11
  58.4 0.2 select_reduce_fusion.1
  58.6 0.1 fusion.35
  58.7 0.5 convolution_convert_fusion.3
  59.2 0.1 all_to_all.16
  59.2 19.0 %all_to_all.24 = bf16[16,5,1152]{2,1,0:T(8,128)(2,1)S(1)} all-to-all(bf16[16,5,1152]{2,1,0:T(8,128)(2,1)S(1)} %all_to_all.16), channel_id=1, replica_groups=mesh['ep'=16,'tp'=2] {'ep'}, dimensions={0} | all-to-all | bytes 368640 | tf_op jit(solution)/shard_map/all_to_all | solution.py:123
  78.3 0.1 all_to_all.18
  78.4 2.1 %all_gather.3 = bf16[80,2304]{1,0:T(8,128)(2,1)S(1)} all-gather(bf16[80,1152]{1,0:T(8,128)(2,1)S(1)} %all_to_all.18), channel_id=1, replica_groups=mesh['ep'=16,'tp'=2] {'tp'}, dimensions={1}, use_global_device_ids=true | all-gather | bytes 552960 | tf_op jit(solution)/shard_map/all_gather | solution.py:124
  80.4 2.2 %fusion.5 = f32[80,512]{1,0:T(8,128)S(1)} fusion(bf16[80,2304]{1,0:T(8,128)(2,1)S(1)} %all_gather.3, bf16[1,2304,512]{2,1,0:T(8,128)(2,1)} %param.32), kind=kOutput, calls=%fused_computation.8 | convolution fusion | flops 188743680 | bytes 2891776 | tf_op jit(solution)/shard_map/dot_general | solution.py:125
  82.6 2.6 %convolution_convert_fusion = bf16[80,2304]{1,0:T(8,128)(2,1)S(1)} fusion(bf16[1,512,2304]{2,1,0:T(8,128)(2,1)S(1)} %copy-done, bf16[80,2304]{1,0:T(8,128)(2,1)S(1)} %all_gather.3, bf16[1,2304,512]{2,1,0:T(8,128)(2,1)} %param.33, f32[80,512]{1,0:T(8,128)S(1)} %fusion.5), kind=kOutput, calls=%fused_computation.2 | convolution fusion | flops 377917440 | bytes 5619712 | tf_op jit(solution)/shard_map/dot_general | solution.py:128
  85.2 1.1 copy.50
  86.3 0.0 reduce-scatter.7.cloned.1.call-update
  86.3 0.0 copy-start.4
  86.3 2.1 %fusion.70 = f32[7,512]{1,0:T(8,128)S(1)} fusion(bf16[7,2304]{1,0:T(8,128)(2,1)S(1)} %fusion.35, bf16[2304,512]{1,0:T(8,128)(2,1)} %param.35), kind=kOutput, calls=%fused_computation.102 | convolution fusion | flops 16515072 | bytes 2405888 | tf_op jit(solution)/shard_map/dot_general | solution.py:93
  88.4 3.9 %reduce-scatter.7.cloned.1.call-done = bf16[1152,80]{1,0:T(8,128)(2,1)} async-done(((bf16[2304,80]{1,0:T(8,128)(2,1)}), bf16[1152,80]{1,0:T(8,128)(2,1)}) %reduce-scatter.7.cloned.1.call-update) | async-done | bytes 184336
  92.3 1.1 copy.51
  93.4 0.8 all_to_all.19
  94.2 6.7 %all-to-all-start.1 = ((bf16[16,5,1152]{2,1,0:T(8,128)(2,1)}), bf16[16,5,1152]{2,1,0:T(8,128)(2,1)S(1)}, u32[]{:S(2)}, u32[]{:S(2)}) async-start(bf16[16,5,1152]{2,1,0:T(8,128)(2,1)} %all_to_all.19), calls=%async_computation.1 | async-start | bytes 589824 | tf_op jit(solution)/shard_map/all_to_all | solution.py:137
  100.9 0.0 reduce-scatter.9.cloned.1.call-start
  101.0 3.2 %convolution_convert_fusion.1 = bf16[7,2304]{1,0:T(8,128)(2,1)S(1)} fusion(bf16[512,2304]{1,0:T(8,128)(2,1)} %param.37, bf16[7,2304]{1,0:T(8,128)(2,1)S(1)} %fusion.35, bf16[2304,512]{1,0:T(8,128)(2,1)} %param.36, f32[7,512]{1,0:T(8,128)S(1)} %fusion.70), kind=kOutput, calls=%fused_computation.3 | convolution fusion | flops 33067776 | bytes 4797440 | tf_op jit(solution)/shard_map/dot_general | solution.py:96
  104.2 1.1 copy.52
  105.3 0.0 reduce-scatter.9.cloned.1.call-update
  105.3 0.1 reduce_sum.70
  105.4 0.1 copy.44
  105.5 0.1 copy.43
  105.6 9.2 %reduce-scatter.9.cloned.1.call-done = bf16[1152,7]{1,0:T(8,128)(2,1)} async-done(((bf16[2304,7]{1,0:T(8,128)(2,1)}), bf16[1152,7]{1,0:T(8,128)(2,1)}) %reduce-scatter.9.cloned.1.call-update) | async-done | bytes 16144
  114.8 1.1 copy.53
  115.9 0.0 all-to-all-done.1
  115.9 0.1 reshape.144
  116.0 0.2 fusion.10
  116.2 0.6 add_convert_fusion
  (29 shorter events, 0.1 us)
Async XLA Ops:
  6.5 76.1 %copy-start = (bf16[1,512,2304]{2,1,0:T(8,128)(2,1)S(1)}, bf16[1,512,2304]{2,1,0:T(8,128)(2,1)}, u32[]{:S(2)}) copy-start(bf16[1,512,2304]{2,1,0:T(8,128)(2,1)} %param.34) | copy-start | bytes 7077892
  6.5 85.7 %reduce-scatter.7.cloned.1.call-start = ((), (), s32[]{:S(2)}) async-start(), calls=%async_computation.4 | async-start | bytes 884736
  11.6 20.6 %copy-start.6 = (s32[7]{0:T(128)S(1)}, s32[7]{0:T(128)}, u32[]{:S(2)}) copy-start(s32[7]{0:T(128)} %param.30) | copy-start | bytes 88
  11.6 20.7 %copy-start.1 = (bf16[7,2304]{1,0:T(8,128)(2,1)S(1)}, bf16[7,2304]{1,0:T(8,128)(2,1)}, u32[]{:S(2)}) copy-start(bf16[7,2304]{1,0:T(8,128)(2,1)} %param.20) | copy-start | bytes 96772
  32.3 11.9 %slice-start = ((s8[4718592]{0:T(1024)(128)(4,1)}), s8[524288]{0:T(1024)(128)(4,1)S(1)}, s32[]{:S(2)}) async-start(s8[4718592]{0:T(1024)(128)(4,1)} %bitcast.88), calls=%async_computation.6 | async-start | bytes 1048576
  35.8 8.2 %copy-start.5 = (f32[8]{0:T(128)S(1)}, f32[8]{0:T(128)}, u32[]{:S(2)}) copy-start(f32[8]{0:T(128)} %param.26) | copy-start | bytes 100
  35.8 8.3 %slice-start.1 = ((s8[4718592]{0:T(1024)(128)(4,1)}), s8[4194304]{0:T(1024)(128)(4,1)S(1)}, s32[]{:S(2)}) async-start(s8[4718592]{0:T(1024)(128)(4,1)} %bitcast.88), calls=%async_computation.7 | async-start | bytes 8388608
  44.2 8.7 %slice-start.2 = ((s8[4718592]{0:T(1024)(128)(4,1)}), s8[4194304]{0:T(1024)(128)(4,1)S(1)}, s32[]{:S(2)}) async-start(s8[4718592]{0:T(1024)(128)(4,1)} %bitcast.90), calls=%async_computation.8 | async-start | bytes 8388608
  44.9 7.8 %copy-start.7 = (bf16[128]{0:T(256)(128)(2,1)S(1)}, bf16[128]{0:T(256)(128)(2,1)}, u32[]{:S(2)}) copy-start(bf16[128]{0:T(256)(128)(2,1)} %param.27) | copy-start | bytes 772
  44.9 7.9 %slice-start.3 = ((s8[4718592]{0:T(1024)(128)(4,1)}), s8[524288]{0:T(1024)(128)(4,1)S(1)}, s32[]{:S(2)}) async-start(s8[4718592]{0:T(1024)(128)(4,1)} %bitcast.90), calls=%async_computation.9 | async-start | bytes 1048576
  52.6 5.6 %copy-start.3 = (bf16[2304]{0:T(1024)(128)(2,1)S(1)}, bf16[2304]{0:T(1024)(128)(2,1)}, u32[]{:S(2)}) copy-start(bf16[2304]{0:T(1024)(128)(2,1)} %param.31) | copy-start | bytes 13828
  52.6 5.6 %copy-start.2 = (s32[7,6]{1,0:T(8,128)S(1)}, s32[7,6]{1,0:T(8,128)}, u32[]{:S(2)}) copy-start(s32[7,6]{1,0:T(8,128)} %param.38) | copy-start | bytes 508
  86.3 19.2 %copy-start.4 = (f32[7,6]{1,0:T(8,128)S(1)}, f32[7,6]{1,0:T(8,128)}, u32[]{:S(2)}) copy-start(f32[7,6]{1,0:T(8,128)} %param.39) | copy-start | bytes 508
  94.2 21.7 %all-to-all-start.1 = ((bf16[16,5,1152]{2,1,0:T(8,128)(2,1)}), bf16[16,5,1152]{2,1,0:T(8,128)(2,1)S(1)}, u32[]{:S(2)}, u32[]{:S(2)}) async-start(bf16[16,5,1152]{2,1,0:T(8,128)(2,1)} %all_to_all.19), calls=%async_computation.1 | async-start | bytes 589824 | tf_op jit(solution)/shard_map/all_to_all | solution.py:137
  100.9 13.8 %reduce-scatter.9.cloned.1.call-start = ((), (), s32[]{:S(2)}) async-start(), calls=%async_computation.5 | async-start | bytes 884736
Sparse Core Ops, SparseCore 0:
  86.4 5.7 reduce-scatter.6
  105.4 9.2 reduce-scatter.8
where the time goes:
time: 125 us; the launch traced here: 124 us
  matrix products  34.1 us (27%)
  local copies, waits for them, and re-layouts  26.8 us (21%)
  blocking collectives  24.9 us (20%)
  between operations  13.7 us (11%)
  waiting for transfers between devices  13.1 us (10%)
  starting transfers between devices  6.78 us (5%)
  other arithmetic  4.34 us (3%)
    unnamed x31, local copies, waits for them, and re-layouts  25.1 us
    all_to_all x1, blocking collectives, shards(): lax.all_to_all(send_slice, 'ep', split_axis=0, concat_axis=0, tiled=True)  19 us
    unnamed x4, waiting for transfers between devices  13.1 us
    dot_general x1, matrix products, shards(): jnp.einsum('shj,sjhv->shv', mixture, cache_values, preferred_element_type...  7.61 us
    dot_general x1, matrix products, shards(): jnp.einsum('shmd,sjhmd->shmj', queries, past_keys, preferred_element_type...  7.34 us
    all_to_all x1, starting transfers between devices, shards(): lax.all_to_all(expert_sum.astype(jnp.bfloat16), 'ep', split_axis=0, conca...  6.73 us
    psum x1, blocking collectives, shards(): lax.psum(attn_part.astype(jnp.bfloat16), 'tp').astype(jnp.float32)  3.78 us
    dot_general x1, matrix products, shards(): jnp.dot(shared_hidden, shared_down, preferred_element_type=jnp.float32)  3.2 us
  transfers between devices with their start and end apart: 3, of which 2 were waited for; matrix products, arithmetic and copies ran while one was open for 6% of the time, Pallas kernels for 0%

commit v1 on v0

--- a/solution.py
+++ b/solution.py
@@ -1,6 +1,9 @@
+import functools
 import jax
 import jax.numpy as jnp
 from jax import lax
+from jax.experimental import pallas as pl
+from jax.experimental.pallas import tpu as pltpu
 from jax.sharding import PartitionSpec as P
 
 epsilon = 1e-06
@@ -15,7 +18,7 @@
     )
 
 
-def shards(
+def plain_shards(
     tokens,
     attn_gain,
     query_weight,
@@ -145,6 +148,380 @@
     return (own_cols.astype(jnp.float32) + routed + shared_out).astype(jnp.bfloat16)
 
 
+BLOCK = 256
+PIECES = 4
+MESH = pl.DeviceIdType.MESH
+NT = (((1,), (1,)), ((), ()))
+
+
+def attend_kernel(
+    lengths_ref, tokens_ref, gain_ref, lambdas_ref, head_gain_ref,
+    wq_hbm, wk_hbm, wv_hbm, wo_hbm, keys_hbm, values_hbm,
+    out_ref,
+    wq, wk, wv, wo, keys, values, q_rows, k_rows, v_rows, head_rows,
+    w_sem, key_sem, value_sem,
+):
+    seqs, width = tokens_ref.shape
+    heads = lambdas_ref.shape[0]
+    head_dim = 64
+    block_rows = BLOCK * heads
+    depth = width // PIECES
+
+    def weight_copy(index, piece):
+        source = (wq_hbm, wk_hbm, wv_hbm, wo_hbm)[index]
+        target = (wq, wk, wv, wo)[index]
+        rows = pl.ds(piece * depth, depth)
+        return pltpu.make_async_copy(source.at[rows], target.at[rows], w_sem.at[index, piece])
+
+    def key_copy(s, b):
+        rows = pl.ds(b * block_rows, block_rows)
+        return pltpu.make_async_copy(keys_hbm.at[s, rows], keys.at[s, rows], key_sem.at[s, b])
+
+    def value_copy(s, b):
+        rows = pl.ds(b * block_rows, block_rows)
+        return pltpu.make_async_copy(values_hbm.at[s, rows], values.at[s, rows], value_sem.at[s, b])
+
+    def block_count(s):
+        return (lengths_ref[s] + (BLOCK - 1)) // BLOCK
+
+    def start_cache(s):
+        @pl.loop(0, block_count(s))
+        def _(b):
+            key_copy(s, b).start()
+            value_copy(s, b).start()
+
+    for index in range(3):
+        for piece in range(PIECES):
+            weight_copy(index, piece).start()
+
+    @pl.loop(0, seqs - 1)
+    def _(s):
+        start_cache(s)
+
+    for piece in range(PIECES):
+        weight_copy(3, piece).start()
+    start_cache(seqs - 1)
+
+    normed = rms_scale(tokens_ref[...], gain_ref[...]).astype(jnp.bfloat16)
+    for index, (weight, rows_ref) in enumerate(((wq, q_rows), (wk, k_rows), (wv, v_rows))):
+        total = None
+        for piece in range(PIECES):
+            weight_copy(index, piece).wait()
+            rows = slice(piece * depth, (piece + 1) * depth)
+            term = jnp.dot(normed[:, rows], weight[rows, :], preferred_element_type=jnp.float32)
+            total = term if total is None else total + term
+        total = total.astype(jnp.bfloat16).astype(jnp.float32)
+        for h in range(heads):
+            rows_ref[0:seqs, h, :] = total[:, h * 128 : (h + 1) * 128]
+
+    scale = head_dim ** (-0.5)
+    lane = lax.broadcasted_iota(jnp.int32, (heads, 128), 1)
+    col = lax.broadcasted_iota(jnp.int32, (2 * heads, block_rows), 1)
+    row = lax.broadcasted_iota(jnp.int32, (2 * heads, block_rows), 0)
+    own_head = lax.rem(col, heads) == lax.rem(row, heads)
+    col = jnp.where(own_head, col, jnp.int32(1 << 30))
+    lam = lambdas_ref[...]
+    head_rows[...] = jnp.zeros_like(head_rows)
+
+    @pl.loop(0, seqs)
+    def _(s):
+        query = q_rows[s]
+        pair = jnp.concatenate(
+            [jnp.where(lane < head_dim, query, 0.0), jnp.where(lane < head_dim, 0.0, query)], axis=0
+        )
+        new_key = k_rows[s]
+        new_value = v_rows[s]
+        peak = (
+            jnp.sum(pair * jnp.concatenate([new_key, new_key], axis=0), axis=1, keepdims=True)
+            * scale
+        )
+        denom = jnp.ones_like(peak)
+        total = jnp.concatenate([new_value, new_value], axis=0)
+        query_pair = pair.astype(jnp.bfloat16)
+
+        def step(b, state):
+            peak, denom, total = state
+            key_copy(s, b).wait()
+            rows = pl.ds(pl.multiple_of(b * block_rows, block_rows), block_rows)
+            scores = (
+                lax.dot_general(query_pair, keys[s, rows], NT, preferred_element_type=jnp.float32)
+                * scale
+            )
+            live = col < (lengths_ref[s] - b * BLOCK) * heads
+            scores = jnp.where(live, scores, -jnp.inf)
+            new_peak = jnp.maximum(peak, jnp.max(scores, axis=1, keepdims=True))
+            fade = jnp.exp(peak - new_peak)
+            terms = jnp.exp(scores - new_peak)
+            value_copy(s, b).wait()
+            denom = denom * fade + jnp.sum(terms, axis=1, keepdims=True)
+            total = total * fade + jnp.dot(
+                terms.astype(jnp.bfloat16), values[s, rows], preferred_element_type=jnp.float32
+            )
+            return new_peak, denom, total
+
+        peak, denom, total = lax.fori_loop(0, block_count(s), step, (peak, denom, total))
+        probs = total / denom
+        head_out = probs[0:heads] - lam * probs[heads:]
+        head_rows[:, s, :] = rms_scale(head_out, head_gain_ref[...])
+
+    flat = jnp.concatenate([head_rows[h] for h in range(heads)], axis=1).astype(jnp.bfloat16)
+    for piece in range(PIECES):
+        weight_copy(3, piece).wait()
+        rows = slice(piece * depth, (piece + 1) * depth)
+        out_ref[:, rows] = lax.dot_general(
+            flat, wo[rows, :], NT, preferred_element_type=jnp.float32
+        ).astype(jnp.bfloat16)
+
+
+def attend(tokens, gain, wq, wk, wv, wo, lambdas, head_gain, cache_keys, cache_values, lengths):
+    seqs, width = tokens.shape
+    heads = lambdas.shape[0]
+    cache_len = cache_keys.shape[1]
+    blocks = cache_len // BLOCK
+    flat = (seqs, cache_len * heads, 128)
+    vmem = pl.BlockSpec(memory_space=pltpu.VMEM)
+    hbm = pl.BlockSpec(memory_space=pl.ANY)
+    return pl.pallas_call(
+        attend_kernel,
+        out_shape=jax.ShapeDtypeStruct((8, width), jnp.bfloat16),
+        in_specs=[pl.BlockSpec(memory_space=pltpu.SMEM)] + [vmem] * 4 + [hbm] * 6,
+        out_specs=vmem,
+        scratch_shapes=[pltpu.VMEM(wq.shape, jnp.bfloat16)] * 4
+        + [pltpu.VMEM(flat, jnp.bfloat16)] * 2
+        + [pltpu.VMEM((8, heads, 128), jnp.float32)] * 3
+        + [pltpu.VMEM((heads, 8, 128), jnp.float32)]
+        + [
+            pltpu.SemaphoreType.DMA((4, PIECES)),
+            pltpu.SemaphoreType.DMA((seqs, blocks)),
+            pltpu.SemaphoreType.DMA((seqs, blocks)),
+        ],
+        compiler_params=pltpu.CompilerParams(vmem_limit_bytes=60 << 20),
+        name="attend",
+    )(
+        lengths, tokens, gain.reshape(1, width), lambdas.reshape(heads, 1),
+        head_gain.reshape(1, 128), wq, wk, wv, wo,
+        cache_keys.reshape(flat), cache_values.reshape(flat),
+    )
+
+
+def experts_kernel(
+    count,
+    part_ref, tokens_ref, gain_ref, ids_ref, weights_ref,
+    gate_hbm, up_hbm, down_hbm, sgate_hbm, sup_hbm, sdown_hbm,
+    out_ref,
+    gate, up, down, sgate, sup, sdown,
+    part_in, mixed, normed, send, arrived, other, give_sum, take_sum, back, returned,
+    give_shared, take_shared,
+    w_sem, pair_send, pair_recv, go_send, go_recv, fill_send, fill_recv, ret_send, ret_recv,
+):
+    seqs, width = tokens_ref.shape
+    slots = send.shape[1]
+    cols = width // 2
+    me = lax.axis_index("ep")
+    half = lax.axis_index("tp")
+    peer = (me, 1 - half)
+    rows_all = count * slots
+    my_cols = pl.ds(pl.multiple_of(half * cols, 128), cols)
+    peer_cols = pl.ds(pl.multiple_of((1 - half) * cols, 128), cols)
+
+    loads = [
+        pltpu.make_async_copy(source, target, w_sem.at[i])
+        for i, (source, target) in enumerate(
+            (
+                (sgate_hbm, sgate), (sup_hbm, sup), (sdown_hbm, sdown),
+                (gate_hbm.at[0], gate), (up_hbm.at[0], up), (down_hbm.at[0], down),
+            )
+        )
+    ]
+    for load in loads:
+        load.start()
+
+    barrier = pltpu.get_barrier_semaphore()
+    pl.semaphore_signal(barrier, inc=1, device_id=peer, device_id_type=MESH)
+    for i in range(1, count):
+        pl.semaphore_signal(
+            barrier, inc=1, device_id=(lax.rem(me + i, count), half), device_id_type=MESH
+        )
+    mixed[...] = jnp.zeros_like(mixed)
+    c_expert = lax.broadcasted_iota(jnp.int32, (seqs, rows_all), 1) // slots
+    c_rank = lax.rem(lax.broadcasted_iota(jnp.int32, (seqs, rows_all), 1), slots)
+    hits = jnp.zeros((seqs, rows_all), jnp.float32)
+    gains = jnp.zeros((seqs, rows_all), jnp.float32)
+    for k in range(ids_ref.shape[1]):
+        same = (ids_ref[:, k : k + 1] == c_expert).astype(jnp.float32)
+        hits = hits + same
+        gains = gains + same * weights_ref[:, k : k + 1]
+    ranks = [jnp.zeros((1, rows_all), jnp.float32)]
+    for t in range(1, seqs):
+        ranks.append(ranks[-1] + hits[t - 1 : t])
+    rank = jnp.concatenate(ranks, axis=0)
+    placed = jnp.where(rank == c_rank.astype(jnp.float32), hits, 0.0)
+    gains = gains * placed
+    pad = jnp.zeros((8 - seqs, rows_all), jnp.float32)
+    spread = jnp.concatenate([placed, pad], axis=0).T.astype(jnp.bfloat16)
+
+    def pair_copy(source, target, i):
+        return pltpu.make_async_remote_copy(
+            src_ref=source, dst_ref=target, send_sem=pair_send.at[i], recv_sem=pair_recv.at[i],
+            device_id=peer, device_id_type=MESH,
+        )
+
+    pl.semaphore_wait(barrier, count)
+    part_copy = pair_copy(part_ref, part_in, 0)
+    part_copy.start()
+    part_copy.wait()
+    attn = part_ref[...].astype(jnp.float32) + part_in[...].astype(jnp.float32)
+    mixed[0:seqs, :] = (
+        (tokens_ref[...].astype(jnp.float32) + attn[0:seqs]).astype(jnp.bfloat16).astype(jnp.float32)
+    )
+    row = rms_scale(mixed[...], gain_ref[...]).astype(jnp.bfloat16)
+    normed[...] = row
+    outgoing = jnp.dot(spread, normed[:, my_cols], preferred_element_type=jnp.float32)
+    for e in range(count):
+        send[e] = outgoing[e * slots : (e + 1) * slots].astype(jnp.bfloat16)
+
+    def go_copy(i):
+        to = lax.rem(me + i, count)
+        return pltpu.make_async_remote_copy(
+            src_ref=send.at[to], dst_ref=arrived.at[me], send_sem=go_send.at[i],
+            recv_sem=go_recv.at[i], device_id=(to, half), device_id_type=MESH,
+        )
+
+    for i in range(1, count):
+        go_copy(i).start()
+    arrived[me] = send[me]
+
+    for load in loads[:3]:
+        load.wait()
+    shared_g = jnp.dot(row, sgate[...], preferred_element_type=jnp.float32)
+    shared_u = jnp.dot(row, sup[...], preferred_element_type=jnp.float32)
+    shared_h = (jax.nn.silu(shared_g) * shared_u).astype(jnp.bfloat16)
+    give_shared[...] = jnp.dot(
+        shared_h, sdown[:, peer_cols], preferred_element_type=jnp.float32
+    ).astype(jnp.bfloat16)
+    shared_copy = pair_copy(give_shared, take_shared, 1)
+    shared_copy.start()
+    shared_own = jnp.dot(shared_h, sdown[:, my_cols], preferred_element_type=jnp.float32)
+    shared_own = shared_own.astype(jnp.bfloat16).astype(jnp.float32)
+
+    def fill_copy(i):
+        source = lax.rem(me - i + count, count)
+        return pltpu.make_async_remote_copy(
+            src_ref=arrived.at[source], dst_ref=other.at[source], send_sem=fill_send.at[i],
+            recv_sem=fill_recv.at[i], device_id=peer, device_id_type=MESH,
+        )
+
+    fill_copy(0).start()
+    for i in range(1, count):
+        go_copy(i).wait()
+        fill_copy(i).start()
+    for load in loads[3:5]:
+        load.wait()
+    mine = arrived[...].astype(jnp.float32).reshape(rows_all, cols).astype(jnp.bfloat16)
+    my_rows = pl.ds(pl.multiple_of(half * cols, 128), cols)
+    peer_rows = pl.ds(pl.multiple_of((1 - half) * cols, 128), cols)
+    gate_out = jnp.dot(mine, gate[my_rows, :], preferred_element_type=jnp.float32)
+    up_out = jnp.dot(mine, up[my_rows, :], preferred_element_type=jnp.float32)
+    for i in range(count):
+        fill_copy(i).wait()
+    theirs = other[...].astype(jnp.float32).reshape(rows_all, cols).astype(jnp.bfloat16)
+    gate_out = gate_out + jnp.dot(theirs, gate[peer_rows, :], preferred_element_type=jnp.float32)
+    up_out = up_out + jnp.dot(theirs, up[peer_rows, :], preferred_element_type=jnp.float32)
+    hidden = (jax.nn.silu(gate_out) * up_out).astype(jnp.bfloat16)
+    loads[5].wait()
+    give_sum[...] = jnp.dot(
+        hidden, down[:, peer_cols], preferred_element_type=jnp.float32
+    ).astype(jnp.bfloat16)
+    sum_copy = pair_copy(give_sum, take_sum, 2)
+    sum_copy.start()
+    own_sum = jnp.dot(hidden, down[:, my_cols], preferred_element_type=jnp.float32)
+    own_sum = own_sum.astype(jnp.bfloat16).astype(jnp.float32)
+    sum_copy.wait()
+    total = own_sum + take_sum[...].astype(jnp.float32)
+    for e in range(count):
+        back[e] = total[e * slots : (e + 1) * slots].astype(jnp.bfloat16)
+
+    def ret_copy(i):
+        to = lax.rem(me + i, count)
+        return pltpu.make_async_remote_copy(
+            src_ref=back.at[to], dst_ref=returned.at[me], send_sem=ret_send.at[i],
+            recv_sem=ret_recv.at[i], device_id=(to, half), device_id_type=MESH,
+        )
+
+    for i in range(1, count):
+        ret_copy(i).start()
+    returned[me] = back[me]
+    shared_copy.wait()
+    result = mixed[:, my_cols] + (shared_own + take_shared[...].astype(jnp.float32))
+    high = gains.astype(jnp.bfloat16)
+    low = (gains - high.astype(jnp.float32)).astype(jnp.bfloat16)
+    for i in range(1, count):
+        ret_copy(i).wait()
+    values = returned[...].astype(jnp.float32).reshape(rows_all, cols).astype(jnp.bfloat16)
+    routed = jnp.dot(high, values, preferred_element_type=jnp.float32) + jnp.dot(
+        low, values, preferred_element_type=jnp.float32
+    )
+    out_ref[...] = (result[0:seqs] + routed).astype(jnp.bfloat16)
+
+
+def run_experts(
+    count, part, tokens, gain, ids, weights, gate, up, down, sgate, sup, sdown
+):
+    seqs, width = tokens.shape
+    capacity = min(seqs, max(2, 2 * seqs * ids.shape[1] // count))
+    slots = -(-capacity // 8) * 8
+    cols = width // 2
+    vmem = pl.BlockSpec(memory_space=pltpu.VMEM)
+    hbm = pl.BlockSpec(memory_space=pl.ANY)
+    half_rows = pltpu.VMEM((count, slots, cols), jnp.bfloat16)
+    flat_rows = pltpu.VMEM((count * slots, cols), jnp.bfloat16)
+    each = pltpu.SemaphoreType.DMA((count,))
+    return pl.pallas_call(
+        functools.partial(experts_kernel, count),
+        out_shape=jax.ShapeDtypeStruct((seqs, cols), jnp.bfloat16),
+        in_specs=[vmem] * 5 + [hbm] * 6,
+        out_specs=vmem,
+        scratch_shapes=[
+            pltpu.VMEM(w.shape[-2:], jnp.bfloat16) for w in (gate, up, down, sgate, sup, sdown)
+        ]
+        + [
+            pltpu.VMEM((8, width), jnp.bfloat16),
+            pltpu.VMEM((8, width), jnp.float32),
+            pltpu.VMEM((8, width), jnp.bfloat16),
+            half_rows, half_rows, half_rows, flat_rows, flat_rows, half_rows, half_rows,
+            pltpu.VMEM((8, cols), jnp.bfloat16),
+            pltpu.VMEM((8, cols), jnp.bfloat16),
+            pltpu.SemaphoreType.DMA((6,)),
+            pltpu.SemaphoreType.DMA((3,)),
+            pltpu.SemaphoreType.DMA((3,)),
+            each, each, each, each, each, each,
+        ],
+        compiler_params=pltpu.CompilerParams(
+            collective_id=0, has_side_effects=True, vmem_limit_bytes=40 << 20
+        ),
+        name="experts",
+    )(part, tokens, gain.reshape(1, width), ids, weights, gate, up, down, sgate, sup, sdown)
+
+
+def fast_shards(
+    tokens, attn_gain, query_weight, key_weight, value_weight, out_weight, lambdas, head_gain,
+    cache_keys, cache_values, lengths, moe_gain, gate_weight, up_weight, down_weight,
+    shared_gate, shared_up, shared_down, expert_ids, expert_weights,
+):
+    part = attend(
+        tokens, attn_gain, query_weight, key_weight, value_weight, out_weight, lambdas, head_gain,
+        cache_keys, cache_values, lengths,
+    )
+    return run_experts(
+        lax.axis_size("ep"), part, tokens, moe_gain, expert_ids, expert_weights,
+        gate_weight, up_weight, down_weight, shared_gate, shared_up, shared_down,
+    )
+
+
+def pick_shards(mesh):
+    return fast_shards if mesh.shape["tp"] == 2 else plain_shards
+
+
 def solution(mesh):
     in_specs = (
         P("ep", None),
@@ -169,4 +546,4 @@
         P("ep", None),
     )
     out_specs = P("ep", "tp")
-    return jax.shard_map(shards, mesh=mesh, in_specs=in_specs, out_specs=out_specs, check_vma=False)
+    return jax.shard_map(pick_shards(mesh), mesh=mesh, in_specs=in_specs, out_specs=out_specs, check_vma=False)

time: 125 us -> 63.3 us (0.51)
  Pallas kernels: 0 us -> 49.9 us
  matrix products: 34.1 us -> 0 us
  blocking collectives: 24.9 us -> 0 us
  local copies, waits for them, and re-layouts: 26.8 us -> 13 us
  between operations: 13.7 us -> 0.09 us
  waiting for transfers between devices: 13.1 us -> 0 us
  starting transfers between devices: 6.78 us -> 0 us
  other arithmetic: 4.34 us -> 0 us
    pallas_call x0 -> x2, Pallas kernels: none -> 49.9 us  [the longest x1 31 us: run_experts(): pl.pallas_call(functools.partial(experts_kernel, count), out_shape=jax.Sh...]
    dot_general x12 -> x0, matrix products: 34.1 us -> none  [the longest x1 7.61 us: shards(): jnp.einsum('shj,sjhv->shv', mixture, cache_values, preferred_element_type...]
    all_to_all x1 -> x0, blocking collectives: 19 us -> none  [shards(): lax.all_to_all(send_slice, 'ep', split_axis=0, concat_axis=0, tiled=True)]
    unnamed x31 -> x21, local copies, waits for them, and re-layouts: 25.1 us -> 9.72 us
    unnamed x4 -> x0, waiting for transfers between devices: 13.1 us -> none
    all_to_all x1 -> x0, starting transfers between devices: 6.73 us -> none  [shards(): lax.all_to_all(expert_sum.astype(jnp.bfloat16), 'ep', split_axis=0, conca...]
    psum x1 -> x0, blocking collectives: 3.78 us -> none  [shards(): lax.psum(attn_part.astype(jnp.bfloat16), 'tp').astype(jnp.float32)]
    reshape x2 -> x3, local copies, waits for them, and re-layouts: 0.19 us -> 3.31 us  [the longest x1 1.31 us: attend(): lambdas.reshape(heads, 1)]
  transfers between devices with their start and end apart: 3 -> 0, of which waited for: 2 -> 0; matrix products, arithmetic and copies ran while one was open for 6% -> 0% of each run, Pallas kernels for 0% -> 0%
where the time goes in v1:
time: 63.3 us; the launch traced here: 63 us
  Pallas kernels  49.9 us (79%)
  local copies, waits for them, and re-layouts  13 us (21%)
    pallas_call x1, Pallas kernels, run_experts(): pl.pallas_call(functools.partial(experts_kernel, count), out_shape=jax.Sh...  31 us
    pallas_call x1, Pallas kernels, attend(): pl.pallas_call(attend_kernel, out_shape=jax.ShapeDtypeStruct((8, width),...  19 us
    unnamed x21, local copies, waits for them, and re-layouts  9.72 us
    reshape x1, local copies, waits for them, and re-layouts, attend(): lambdas.reshape(heads, 1)  1.31 us
    reshape x1, local copies, waits for them, and re-layouts, attend(): gain.reshape(1, width)  1.3 us

profile of v1, /device:TPU:0, one launch (start us, length us, event | category | flops | bytes accessed | tf_op | source)
XLA Modules:
  0.0 63.0 jit_solution(2500325129409035475)
XLA Ops:
  0.0 1.3 %copy.21.lambdas_ref = f32[8,1]{1,0:T(8,128)} copy(f32[8,1]{0,1:T(1,128)} %bitcast.7) | data formatting | bytes 64 | tf_op jit(solution)/shard_map/reshape | solution.py:301
  1.3 1.3 %reshape.18.gain_ref = bf16[1,2304]{1,0:T(2,128)(2,1)} reshape(bf16[2304]{0:T(1024)(128)(2,1)} %param.21) | data formatting | bytes 9216 | tf_op jit(solution)/shard_map/reshape | solution.py:301
  2.6 0.7 %reshape.23.gain_ref = bf16[1,2304]{1,0:T(2,128)(2,1)S(1)} reshape(bf16[2304]{0:T(1024)(128)(2,1)} %param.31) | data formatting | bytes 9216 | tf_op jit(solution)/shard_map/reshape | solution.py:503
  3.3 0.0 copy-start
  3.3 0.0 copy-start.6
  3.3 0.0 copy-start.8
  3.3 0.0 copy-start.9
  3.4 19.0 %attend.1.part_ref = bf16[8,2304]{1,0:T(8,128)(2,1)} custom-call(s32[7]{0:T(128)} %lengths_ref.1, bf16[7,2304]{1,0:T(8,128)(2,1)} %tokens_ref.3, bf16[1,2304]{1,0:T(2,128)(2,1)} %reshape.18.gain_ref, f32[8,1]{1,0:T(8,128)} %copy.21.lambdas_ref, bf16[1,128]{1,0:T(2,128)(2,1)} %bitcast.6, bf16[2304,1024]{1,0:T(8,128)(2,1)} %wq_hbm.1, ...), custom_call_target="tpu_custom_call" | custom-call | tf_op jit(solution)/shard_map/attend/pallas_call | solution.py:284
  22.3 0.0 copy-done
  22.3 0.0 copy-done.6
  22.3 0.0 copy-done.8
  22.4 0.0 copy-done.9
  22.4 0.0 copy-start.1
  22.4 1.7 %copy-done.1 = bf16[1,2304,512]{2,1,0:T(8,128)(2,1)S(1)} copy-done((bf16[1,2304,512]{2,1,0:T(8,128)(2,1)S(1)}, bf16[1,2304,512]{2,1,0:T(8,128)(2,1)}, u32[]{:S(2)}) %copy-start.1) | copy-done | bytes 2359320
  24.0 0.0 copy-start.2
  24.0 1.7 %copy-done.2 = bf16[1,512,2304]{2,1,0:T(8,128)(2,1)S(1)} copy-done((bf16[1,512,2304]{2,1,0:T(8,128)(2,1)S(1)}, bf16[1,512,2304]{2,1,0:T(8,128)(2,1)}, u32[]{:S(2)}) %copy-start.2) | copy-done | bytes 2359320
  25.7 0.0 copy-start.3
  25.7 1.7 %copy-done.3 = bf16[2304,512]{1,0:T(8,128)(2,1)S(1)} copy-done((bf16[2304,512]{1,0:T(8,128)(2,1)S(1)}, bf16[2304,512]{1,0:T(8,128)(2,1)}, u32[]{:S(2)}) %copy-start.3) | copy-done | bytes 2359320
  27.4 0.0 copy-start.4
  27.4 1.7 %copy-done.4 = bf16[2304,512]{1,0:T(8,128)(2,1)S(1)} copy-done((bf16[2304,512]{1,0:T(8,128)(2,1)S(1)}, bf16[2304,512]{1,0:T(8,128)(2,1)}, u32[]{:S(2)}) %copy-start.4) | copy-done | bytes 2359320
  29.0 0.0 copy-start.5
  29.0 1.7 %copy-done.5 = bf16[512,2304]{1,0:T(8,128)(2,1)S(1)} copy-done((bf16[512,2304]{1,0:T(8,128)(2,1)S(1)}, bf16[512,2304]{1,0:T(8,128)(2,1)}, u32[]{:S(2)}) %copy-start.5) | copy-done | bytes 2359320
  30.7 0.0 copy-start.7
  30.7 0.8 %copy-done.7 = bf16[8,2304]{1,0:T(8,128)(2,1)S(1)} copy-done((bf16[8,2304]{1,0:T(8,128)(2,1)S(1)}, bf16[8,2304]{1,0:T(8,128)(2,1)}, u32[]{:S(2)}) %copy-start.7) | copy-done | bytes 36888
  31.5 31.0 %experts.1 = bf16[7,1152]{1,0:T(8,128)(2,1)S(1)} custom-call(bf16[8,2304]{1,0:T(8,128)(2,1)S(1)} %copy-done.7, bf16[7,2304]{1,0:T(8,128)(2,1)S(1)} %copy-done.6, bf16[1,2304]{1,0:T(2,128)(2,1)S(1)} %reshape.23.gain_ref, s32[7,6]{1,0:T(8,128)S(1)} %copy-done.8, f32[7,6]{1,0:T(8,128)S(1)} %copy-done.9, bf16[1,2304,512]{2,1,0:T(8,128)(2,1)S(1)} %copy-done, ...), custom_call_target="tpu_custom_call" | custom-call | tf_op jit(solution)/shard_map/experts/pallas_call | solution.py:479
  62.4 0.6 copy.23
Async XLA Ops:
  3.3 19.0 %copy-start = (bf16[1,2304,512]{2,1,0:T(8,128)(2,1)S(1)}, bf16[1,2304,512]{2,1,0:T(8,128)(2,1)}, u32[]{:S(2)}) copy-start(bf16[1,2304,512]{2,1,0:T(8,128)(2,1)} %gate_hbm.1) | copy-start | bytes 7077892
  3.3 19.0 %copy-start.6 = (bf16[7,2304]{1,0:T(8,128)(2,1)S(1)}, bf16[7,2304]{1,0:T(8,128)(2,1)}, u32[]{:S(2)}) copy-start(bf16[7,2304]{1,0:T(8,128)(2,1)} %tokens_ref.3) | copy-start | bytes 96772
  3.3 19.0 %copy-start.8 = (s32[7,6]{1,0:T(8,128)S(1)}, s32[7,6]{1,0:T(8,128)}, u32[]{:S(2)}) copy-start(s32[7,6]{1,0:T(8,128)} %ids_ref.1) | copy-start | bytes 508
  3.3 19.0 %copy-start.9 = (f32[7,6]{1,0:T(8,128)S(1)}, f32[7,6]{1,0:T(8,128)}, u32[]{:S(2)}) copy-start(f32[7,6]{1,0:T(8,128)} %weights_ref.1) | copy-start | bytes 508
  22.4 1.7 %copy-start.1 = (bf16[1,2304,512]{2,1,0:T(8,128)(2,1)S(1)}, bf16[1,2304,512]{2,1,0:T(8,128)(2,1)}, u32[]{:S(2)}) copy-start(bf16[1,2304,512]{2,1,0:T(8,128)(2,1)} %up_hbm.1) | copy-start | bytes 7077892
  24.0 1.7 %copy-start.2 = (bf16[1,512,2304]{2,1,0:T(8,128)(2,1)S(1)}, bf16[1,512,2304]{2,1,0:T(8,128)(2,1)}, u32[]{:S(2)}) copy-start(bf16[1,512,2304]{2,1,0:T(8,128)(2,1)} %down_hbm.1) | copy-start | bytes 7077892
  25.7 1.7 %copy-start.3 = (bf16[2304,512]{1,0:T(8,128)(2,1)S(1)}, bf16[2304,512]{1,0:T(8,128)(2,1)}, u32[]{:S(2)}) copy-start(bf16[2304,512]{1,0:T(8,128)(2,1)} %sgate_hbm.1) | copy-start | bytes 7077892
  27.4 1.7 %copy-start.4 = (bf16[2304,512]{1,0:T(8,128)(2,1)S(1)}, bf16[2304,512]{1,0:T(8,128)(2,1)}, u32[]{:S(2)}) copy-start(bf16[2304,512]{1,0:T(8,128)(2,1)} %sup_hbm.1) | copy-start | bytes 7077892
  29.0 1.7 %copy-start.5 = (bf16[512,2304]{1,0:T(8,128)(2,1)S(1)}, bf16[512,2304]{1,0:T(8,128)(2,1)}, u32[]{:S(2)}) copy-start(bf16[512,2304]{1,0:T(8,128)(2,1)} %sdown_hbm.1) | copy-start | bytes 7077892
  30.7 0.8 %copy-start.7 = (bf16[8,2304]{1,0:T(8,128)(2,1)S(1)}, bf16[8,2304]{1,0:T(8,128)(2,1)}, u32[]{:S(2)}) copy-start(bf16[8,2304]{1,0:T(8,128)(2,1)} %attend.1.part_ref) | copy-start | bytes 110596

commit v2 on v1

--- a/solution.py
+++ b/solution.py
@@ -202,7 +202,7 @@
         weight_copy(3, piece).start()
     start_cache(seqs - 1)
 
-    normed = rms_scale(tokens_ref[...], gain_ref[...]).astype(jnp.bfloat16)
+    normed = rms_scale(tokens_ref[...], gain_ref[...].astype(jnp.float32).reshape(1, width)).astype(jnp.bfloat16)
     for index, (weight, rows_ref) in enumerate(((wq, q_rows), (wk, k_rows), (wv, v_rows))):
         total = None
         for piece in range(PIECES):
@@ -220,7 +220,10 @@
     row = lax.broadcasted_iota(jnp.int32, (2 * heads, block_rows), 0)
     own_head = lax.rem(col, heads) == lax.rem(row, heads)
     col = jnp.where(own_head, col, jnp.int32(1 << 30))
-    lam = lambdas_ref[...]
+    head_at = lax.broadcasted_iota(jnp.int32, (heads, 1), 0)
+    lam = jnp.zeros((heads, 1), jnp.float32)
+    for h in range(heads):
+        lam = jnp.where(head_at == h, lambdas_ref[h], lam)
     head_rows[...] = jnp.zeros_like(head_rows)
 
     @pl.loop(0, seqs)
@@ -280,11 +283,12 @@
     blocks = cache_len // BLOCK
     flat = (seqs, cache_len * heads, 128)
     vmem = pl.BlockSpec(memory_space=pltpu.VMEM)
-    hbm = pl.BlockSpec(memory_space=pl.ANY)
+    smem = pl.BlockSpec(memory_space=pltpu.SMEM)
+    hbm = pl.BlockSpec(memory_space=pltpu.HBM)
     return pl.pallas_call(
         attend_kernel,
         out_shape=jax.ShapeDtypeStruct((8, width), jnp.bfloat16),
-        in_specs=[pl.BlockSpec(memory_space=pltpu.SMEM)] + [vmem] * 4 + [hbm] * 6,
+        in_specs=[smem, vmem, vmem, smem, vmem] + [hbm] * 6,
         out_specs=vmem,
         scratch_shapes=[pltpu.VMEM(wq.shape, jnp.bfloat16)] * 4
         + [pltpu.VMEM(flat, jnp.bfloat16)] * 2
@@ -298,7 +302,7 @@
         compiler_params=pltpu.CompilerParams(vmem_limit_bytes=60 << 20),
         name="attend",
     )(
-        lengths, tokens, gain.reshape(1, width), lambdas.reshape(heads, 1),
+        lengths, tokens, gain, lambdas,
         head_gain.reshape(1, 128), wq, wk, wv, wo,
         cache_keys.reshape(flat), cache_values.reshape(flat),
     )
@@ -374,7 +378,7 @@
     mixed[0:seqs, :] = (
         (tokens_ref[...].astype(jnp.float32) + attn[0:seqs]).astype(jnp.bfloat16).astype(jnp.float32)
     )
-    row = rms_scale(mixed[...], gain_ref[...]).astype(jnp.bfloat16)
+    row = rms_scale(mixed[...], gain_ref[...].astype(jnp.float32).reshape(1, width)).astype(jnp.bfloat16)
     normed[...] = row
     outgoing = jnp.dot(spread, normed[:, my_cols], preferred_element_type=jnp.float32)
     for e in range(count):
@@ -472,7 +476,7 @@
     slots = -(-capacity // 8) * 8
     cols = width // 2
     vmem = pl.BlockSpec(memory_space=pltpu.VMEM)
-    hbm = pl.BlockSpec(memory_space=pl.ANY)
+    hbm = pl.BlockSpec(memory_space=pltpu.HBM)
     half_rows = pltpu.VMEM((count, slots, cols), jnp.bfloat16)
     flat_rows = pltpu.VMEM((count * slots, cols), jnp.bfloat16)
     each = pltpu.SemaphoreType.DMA((count,))
@@ -497,10 +501,10 @@
             each, each, each, each, each, each,
         ],
         compiler_params=pltpu.CompilerParams(
-            collective_id=0, has_side_effects=True, vmem_limit_bytes=40 << 20
+            collective_id=0, has_side_effects=True, vmem_limit_bytes=60 << 20
         ),
         name="experts",
-    )(part, tokens, gain.reshape(1, width), ids, weights, gate, up, down, sgate, sup, sdown)
+    )(part, tokens, gain, ids, weights, gate, up, down, sgate, sup, sdown)
 
 
 def fast_shards(

time: 63.3 us -> 50.2 us (0.79)
  local copies, waits for them, and re-layouts: 13 us -> 1.33 us
  Pallas kernels: 49.9 us -> 48.9 us
    unnamed x21 -> x1, local copies, waits for them, and re-layouts: 9.72 us -> 1.33 us
    reshape x3 -> x0, local copies, waits for them, and re-layouts: 3.31 us -> none  [the longest x1 1.31 us: attend(): lambdas.reshape(heads, 1)]
where the time goes in v2:
time: 50.2 us
  Pallas kernels  48.9 us (97%)
  local copies, waits for them, and re-layouts  1.33 us (3%)
    pallas_call x1, Pallas kernels, run_experts(): pl.pallas_call(functools.partial(experts_kernel, count), out_shape=jax.Sh...  30.5 us
    pallas_call x1, Pallas kernels, attend(): pl.pallas_call(attend_kernel, out_shape=jax.ShapeDtypeStruct((8, width),...  18.4 us
    unnamed x1, local copies, waits for them, and re-layouts  1.33 us

profile of v2, /device:TPU:0, one launch (start us, length us, event | category | flops | bytes accessed | tf_op | source)
XLA Modules:
  0.0 50.2 jit_solution(929862905978064777)
XLA Ops:
  0.0 18.4 %attend.1.part_ref = bf16[8,2304]{1,0:T(8,128)(2,1)} custom-call(s32[7]{0:T(128)} %lengths_ref.1, bf16[7,2304]{1,0:T(8,128)(2,1)} %tokens_ref.3, bf16[2304]{0:T(1024)(128)(2,1)} %gain_ref.2, f32[8]{0:T(128)} %lambdas_ref.1, bf16[1,128]{1,0:T(2,128)(2,1)} %bitcast.5, bf16[2304,1024]{1,0:T(8,128)(2,1)} %wq_hbm.1, bf16[2304,1024]{1,0:T(8,128)(2,1)} %wk_hbm.1, ...), custom_call_target="tpu_custom_call" | custom-call | tf_op jit(solution)/shard_map/attend/pallas_call | solution.py:288
  18.4 30.5 %experts.1 = bf16[7,1152]{1,0:T(8,128)(2,1)} custom-call(bf16[8,2304]{1,0:T(8,128)(2,1)} %attend.1.part_ref, bf16[7,2304]{1,0:T(8,128)(2,1)} %tokens_ref.3, bf16[2304]{0:T(1024)(128)(2,1)} %gain_ref.3, s32[7,6]{1,0:T(8,128)} %ids_ref.1, f32[7,6]{1,0:T(8,128)} %weights_ref.1, bf16[1,2304,512]{2,1,0:T(8,128)(2,1)} %gate_hbm.1, bf16[1,2304,512]{2,1,0:T(8,128)(2,1)} %up_hbm.1, ...), custom_call_target="tpu_custom_call" | custom-call | tf_op jit(solution)/shard_map/experts/pallas_call | solution.py:483
  48.9 1.3 %copy.22 = bf16[7,1152]{1,0:T(8,128)(2,1)} copy(bf16[7,1152]{1,0:T(8,128)(2,1)} %experts.1) | data formatting | bytes 32256
